TPU v7x, 512 devices: a whole 4x8x8 slice. The times are simulated.
512 devices in a mesh: dp: 4 (over x), kv: 64 (over z, y), tp: 2 (over core).
Axes of the slice: x: 4, y: 8, z: 8, core: 2. Of those that a mesh axis runs over, the one named last changes fastest.
Arguments:
- tokens: bfloat16 [512, 4, 4096], P('dp', None, 'kv'), may hold values from -260 to 260
- norm_gain: bfloat16 [4096], replicated, may hold values from 0.099609375 to 1.8984375
- query_weight: bfloat16 [4096, 2048], P(None, ('tp', 'kv')), may hold values from -0.09375 to 0.09375
- key_weight: bfloat16 [4096, 2048], P(None, ('tp', 'kv')), may hold values from -0.09375 to 0.09375
- value_weight: bfloat16 [4096, 4096], P(None, ('tp', 'kv')), may hold values from -0.09375 to 0.09375
- gate_weight: bfloat16 [4096, 4096], P(None, ('tp', 'kv')), may hold values from -0.09375 to 0.09375
- out_weight: bfloat16 [4096, 4096], P('tp', 'kv'), may hold values from -0.09375 to 0.09375
- decay_rate: float32 [16], P('tp'), may hold values from 0.02 to 1
- prior_state: float32 [512, 16, 128, 256], P(('dp', 'kv'), 'tp'), may hold values from -0.6 to 0.6
- last_keys: bfloat16 [512, 4, 16, 128], P(('dp', 'kv'), None, 'tp'), may hold values from -0.5390625 to 0.5390625
- last_values: bfloat16 [512, 4, 16, 256], P(('dp', 'kv'), None, 'tp'), may hold values from -6 to 6
- accepted: int32 [512], P(('dp', 'kv')), may hold values from 0 to 4
- lengths: int32 [512], P(('dp', 'kv')), may hold values from 16 to 99999
Outputs:
- retained: bfloat16 [512, 4, 4096], P('dp', None, ('kv', 'tp'))
- new_state: float32 [512, 16, 128, 256], P(('dp', 'kv'), 'tp')
- new_keys: bfloat16 [512, 4, 16, 128], P(('dp', 'kv'), None, 'tp')
- new_values: bfloat16 [512, 4, 16, 256], P(('dp', 'kv'), None, 'tp')
Inputs may be any that keep to these rules, and one draw needn't show every extreme that they name: `accepted`: how many of the last step's 4 proposals were taken.
All inputs are finite; a program needn't handle non-finite values.
Results may differ from a plain program's by a relative error of at most 0.012.
Values may be sent and summed in bfloat16 or wider, within the bound.
No kernel may reach another device: no remote copies, remote signals or barrier semaphores. Data moves between devices by JAX's collectives and lax.ppermute only.
A program may use at most 64 MiB of HBM per device.

v0:
```python
import jax
import jax.numpy as jnp
from jax import lax
from jax.sharding import Mesh
from jax.sharding import PartitionSpec as P

KV = ("kv_0", "kv_1")
TP_KV = ("tp", "kv_0", "kv_1")
DP_KV = ("dp", "kv_0", "kv_1")
KV_TP = ("kv_0", "kv_1", "tp")
epsilon = 1e-06


def over_axes(value, axes):
    for axis in axes:
        value = lax.psum(value, axis)
    return value


def swapped(value, axis, bit):
    return lax.ppermute(value, axis, [(i, i ^ 1 << bit) for i in range(lax.axis_size(axis))])


def laid_out(blocks, dim):
    lengths = list(blocks.shape[1:])
    lengths[dim] *= blocks.shape[0]
    return jnp.moveaxis(blocks, 0, dim).reshape(lengths)


def stacked_from(value, axes, turns):
    blocks = value[None]
    for k in turns:
        blocks = lax.all_gather(blocks, axes[k], axis=0, tiled=True)
    carried = [lax.axis_size(axes[k]) for k in reversed(turns)]
    blocks = blocks.reshape(*carried, *value.shape)
    turned = sorted(range(len(turns)), key=lambda place: turns[len(turns) - 1 - place])
    return blocks.transpose(*turned, *range(len(turns), blocks.ndim)).reshape(-1, *value.shape)


def gathered_by_axis(value, axes, turns, dim):
    return laid_out(stacked_from(value, axes, turns), dim)


def in_blocks(value, dim, length):
    before, after = (value.shape[:dim], value.shape[dim + 1 :])
    return jnp.moveaxis(value.reshape(*before, length, -1, *after), dim, 0)


def summed_on_arrival(value, axis, dim):
    length = lax.axis_size(axis)
    blocks = lax.all_to_all(in_blocks(value, dim, length), axis, 0, 0, tiled=True)
    return jnp.sum(blocks.astype(jnp.float32), axis=0)


def rotate(field_in, positions):
    half_size = field_in.shape[-1] // 2
    frequency = jnp.power(10000.0, -jnp.arange(half_size, dtype=jnp.float32) / half_size)
    angles = positions.astype(jnp.float32)[:, :, None, None] * frequency
    cosine, sine_part = (jnp.cos(angles), jnp.sin(angles))
    floats = field_in.astype(jnp.float32)
    first_half, second = (floats[..., :half_size], floats[..., half_size:])
    return jnp.concatenate(
        [first_half * cosine - second * sine_part, first_half * sine_part + second * cosine],
        axis=-1,
    )


def retain(
    query_rot, key_rot, value_rows, prior_state, last_keys, last_values, accepted, log_decay
):
    highest = lax.Precision.HIGHEST
    proposals = query_rot.shape[1]
    step_ids = jnp.arange(proposals, dtype=jnp.int32)
    taken_mask = step_ids[None, :] < accepted[:, None]
    power_exp = jnp.maximum(accepted[:, None] - 1 - step_ids[None, :], 0).astype(jnp.float32)
    weight = jnp.where(
        taken_mask[:, :, None], jnp.exp(log_decay[None, None, :] * power_exp[:, :, None]), 0.0
    )
    carried = jnp.exp(log_decay[None, :] * accepted[:, None].astype(jnp.float32))
    weighted_keys = last_keys.astype(jnp.float32) * weight[..., None]
    taken_state = carried[:, :, None, None] * prior_state + jnp.einsum(
        "sphd,sphe->shde", weighted_keys, last_values.astype(jnp.float32), precision=highest
    )
    scores = jnp.einsum(
        "sthd,smhd->shtm",
        query_rot.astype(jnp.float32),
        key_rot.astype(jnp.float32),
        precision=highest,
    )
    offset = (step_ids[:, None] - step_ids[None, :]).astype(jnp.float32)
    decay_grid = jnp.where(
        offset[None] >= 0.0, jnp.exp(log_decay[:, None, None] * jnp.maximum(offset, 0.0)[None]), 0.0
    )
    inner_sum = jnp.einsum(
        "shtm,smhe->sthe",
        scores * decay_grid[None],
        value_rows.astype(jnp.float32),
        precision=highest,
    )
    query_decay = jnp.exp(log_decay[None, :] * (step_ids[:, None].astype(jnp.float32) + 1.0))
    cross_sum = jnp.einsum(
        "sthd,shde->sthe",
        query_rot.astype(jnp.float32) * query_decay[None, :, :, None],
        taken_state,
        precision=highest,
    )
    return (inner_sum + cross_sum, taken_state)


def row_scale(tokens, row_block, first_row):
    partial_sq = jnp.sum(jnp.square(tokens.astype(jnp.float32)), axis=-1)
    total_sq = over_axes(partial_sq, KV)
    picked = lax.dynamic_slice_in_dim(total_sq, first_row, row_block.shape[1], 1)
    return lax.rsqrt(picked / row_block.shape[-1] + epsilon)


def shards(
    tokens,
    norm_gain,
    query_weight,
    key_weight,
    value_weight,
    gate_weight,
    out_weight,
    decay_rate,
    prior_state,
    last_keys,
    last_values,
    accepted,
    lengths,
):
    groups = lax.axis_size(KV)
    owned_seqs, proposals, _ = tokens.shape
    local_seqs, heads_here, key_size, value_size = prior_state.shape
    width = norm_gain.shape[0]
    key_cols = query_weight.shape[1]
    value_cols = value_weight.shape[1]
    col_span = 2 * key_cols + 2 * value_cols
    gain_vector = norm_gain.astype(jnp.float32)
    pair_index = lax.axis_index("tp")
    half_props = proposals // 2
    own_half = lax.dynamic_slice_in_dim(tokens, pair_index * half_props, half_props, 1)
    gathered = lax.all_gather(own_half, KV, axis=2, tiled=True)
    row_total = gathered.shape[0] * gathered.shape[1]
    scaled = (
        gathered.astype(jnp.float32)
        * row_scale(tokens, gathered, pair_index * half_props)[..., None]
        * gain_vector
    )
    normed = scaled.astype(jnp.bfloat16).reshape(row_total, width)
    own_weights = jnp.concatenate([query_weight, key_weight, value_weight, gate_weight], axis=1)
    other_weights = swapped(own_weights, "tp", 0)
    both_weights = jnp.where(
        pair_index == 0,
        jnp.concatenate([own_weights, other_weights], axis=1),
        jnp.concatenate([other_weights, own_weights], axis=1),
    )
    columns = jnp.dot(normed, both_weights, preferred_element_type=jnp.float32).astype(jnp.bfloat16)
    columns = columns.reshape(owned_seqs, half_props, 2 * col_span)
    arrived = lax.all_to_all(columns, KV, split_axis=0, concat_axis=2, tiled=True)
    arrived = arrived.reshape(local_seqs, half_props, groups, 2 * col_span)
    lower_part = arrived[..., :col_span]
    upper_part = arrived[..., col_span:]
    kept_part = jnp.where(pair_index == 0, lower_part, upper_part)
    sent_part = jnp.where(pair_index == 0, upper_part, lower_part)
    received = swapped(sent_part, "tp", 0)
    assembled = jnp.where(
        pair_index == 0,
        jnp.concatenate([kept_part, received], axis=1),
        jnp.concatenate([received, kept_part], axis=1),
    )

    def role_rows(first_col, col_count, last_size):
        picked = assembled[..., first_col : first_col + col_count]
        return picked.reshape(local_seqs, proposals, heads_here, last_size)

    query_rows = role_rows(0, key_cols, key_size)
    key_rows = role_rows(key_cols, key_cols, key_size)
    value_rows = role_rows(2 * key_cols, value_cols, value_size)
    gate_rows = role_rows(2 * key_cols + value_cols, value_cols, value_size)
    positions = (lengths + accepted)[:, None] + jnp.arange(proposals, dtype=jnp.int32)[None, :]
    query_rot = rotate(query_rows, positions).astype(jnp.bfloat16)
    key_rot = (rotate(key_rows, positions) * key_size ** (-0.5)).astype(jnp.bfloat16)
    heads_out, taken_state = retain(
        query_rot, key_rot, value_rows, prior_state, last_keys, last_values, accepted, -decay_rate
    )
    head_norm = heads_out * lax.rsqrt(
        jnp.mean(heads_out * heads_out, axis=-1, keepdims=True) + epsilon
    )
    gated = (jax.nn.silu(gate_rows.astype(jnp.float32)) * head_norm).astype(jnp.bfloat16)
    gated = gated.reshape(local_seqs, proposals, heads_here * value_size)
    gathered_piece = gathered_by_axis(gated, KV, (0, 1), 0)
    piece_rows = gathered_piece.shape[0]
    flat_rows = gathered_piece.reshape(piece_rows * proposals, heads_here * value_size)
    product = jnp.dot(flat_rows, out_weight, preferred_element_type=jnp.float32)
    partial_terms = product.reshape(piece_rows, proposals, out_weight.shape[1])
    retained = summed_on_arrival(partial_terms.astype(jnp.bfloat16), "tp", 2).astype(jnp.bfloat16)
    return (retained, taken_state, key_rot, value_rows)


def solution(mesh):
    finer = Mesh(
        mesh.devices.reshape(mesh.shape["dp"], 8, 8, mesh.shape["tp"]), ("dp", "kv_0", "kv_1", "tp")
    )
    return jax.shard_map(
        shards,
        mesh=finer,
        in_specs=(
            P("dp", None, KV),
            P(),
            P(None, TP_KV),
            P(None, TP_KV),
            P(None, TP_KV),
            P(None, TP_KV),
            P("tp", KV),
            P("tp"),
            P(DP_KV, "tp", None, None),
            P(DP_KV, None, "tp", None),
            P(DP_KV, None, "tp", None),
            P(DP_KV),
            P(DP_KV),
        ),
        out_specs=(
            P("dp", None, KV_TP),
            P(DP_KV, "tp", None, None),
            P(DP_KV, None, "tp", None),
            P(DP_KV, None, "tp", None),
        ),
        check_vma=False,
    )
```

profile of v0, /device:TPU:1, one launch (start us, length us, event | category | flops | bytes accessed | tf_op | source)
XLA Modules:
  0.0 229.2 jit_solution(18437961642913602430)
XLA Ops:
  7.3 1.6 constant_dynamic-slice_fusion
  8.9 2.0 pad_maximum_fusion
  11.0 8.7 %collective-permute-start = (bf16[4096,96]{0,1:T(8,128)(2,1)}, bf16[4096,96]{0,1:T(8,128)(2,1)}, u32[]{:S(2)}, u32[]{:S(2)}) collective-permute-start(bf16[4096,96]{0,1:T(8,128)(2,1)} %pad_maximum_fusion), channel_id=1, source_target_pairs={{0,1},{1,0},{2,3},{3,2},{4,5},{5,4},{6,7},{7,6},{8,9},{9,8},{10,11... | collective-permute-start | bytes 2359304 | tf_op jit(solution)/shard_map/ppermute | solution.py:21
  21.0 14.1 %psum.14 = f32[128,4]{0,1:T(4,128)S(1)} all-reduce(f32[128,4]{0,1:T(4,128)S(1)} %multiply_reduce_fusion), channel_id=1, replica_groups=mesh['dp'=4,'kv_0'=8,'kv_1'=8,'tp'=2] {'kv_0'}, use_global_device_ids=true, to_apply=%region_1.0 | all-reduce | flops 512 | bytes 4096 | tf_op jit(solution)/shard_map/psum | solution.py:16
  35.1 15.0 %psum.15 = f32[128,4]{0,1:T(4,128)S(1)} all-reduce(f32[128,4]{0,1:T(4,128)S(1)} %psum.14), channel_id=1, replica_groups=mesh['dp'=4,'kv_0'=8,'kv_1'=8,'tp'=2] {'kv_1'}, use_global_device_ids=true, to_apply=%region_2.0 | all-reduce | flops 512 | bytes 4096 | tf_op jit(solution)/shard_map/psum | solution.py:16
  51.5 2.8 %multiply_add_fusion = f32[2,8,128,256]{3,2,1,0:T(8,128)S(1)} fusion(f32[2,8,128,256]{3,2,1,0:T(8,128)} %param.21, f32[2,8]{1,0:T(2,128)S(1)} %multiply_exponential_fusion.1, bf16[2,4,8,256]{3,2,1,0:T(8,128)(2,1)S(1)} %copy-done.8, f32[2,4,8,128]{3,2,1,0:T(8,128)S(1)} %convert_multiply_fusion), kind=kOutput, calls=%fused_computation.2 | convolution fusion | flops 26214400 | bytes 4259904 | tf_op jit(solution)/shard_map/sphd,sphe->shde/dot_general | solution.py:81
  55.2 2.5 %constant_dynamic-update-slice_fusion.9 = (bf16[4096,192]{0,1:T(8,128)(2,1)}, bf16[4096,192]{0,1:T(8,128)(2,1)}) fusion(bf16[4096,96]{0,1:T(8,128)(2,1)} %collective-permute-done, bf16[4096,192]{0,1:T(8,128)(2,1)} %constant_dynamic-update-slice_fusion.1), kind=kLoop, calls=%fused_computation.49 | loop fusion | bytes 2359296
  60.4 36.0 %all-gather.3.cloned.1.call-done = bf16[128,2,4096]{0,2,1:T(8,128)(2,1)} async-done(((bf16[128,2,64]{0,2,1:T(8,128)(2,1)}), bf16[128,2,4096]{0,2,1:T(8,128)(2,1)}) %all-gather.3.cloned.1.call-update) | async-done | bytes 2097168 | tf_op jit(solution)/shard_map/all_gather | solution.py:143
  96.4 2.9 %multiply_convert_fusion = bf16[128,2,4096]{0,2,1:T(8,128)(2,1)} fusion(bf16[128,2,4096]{0,2,1:T(8,128)(2,1)} %all-gather.3.cloned.1.call-done, f32[4096]{0:T(1024)S(1)} %convert_element_type.96, f32[128,2]{0,1:T(2,128)S(1)} %add_rsqrt_fusion.1), kind=kLoop, calls=%fused_computation | loop fusion | flops 4194304 | bytes 4211712 | tf_op jit(solution)/shard_map/convert_element_type | solution.py:150
  99.3 6.2 %copy.63 = bf16[128,2,4096]{2,1,0:T(2,128)(2,1)} copy(bf16[128,2,4096]{0,2,1:T(8,128)(2,1)} %multiply_convert_fusion) | data formatting | bytes 4194304 | tf_op jit(solution)/shard_map/convert_element_type | solution.py:150
  105.5 4.1 %reshape.228 = bf16[256,4096]{1,0:T(8,128)(2,1)} reshape(bf16[128,2,4096]{2,1,0:T(2,128)(2,1)} %copy.63) | data formatting | bytes 4194304 | tf_op jit(solution)/shard_map/reshape | solution.py:150
  109.7 2.9 %fusion.3 = bf16[256,192]{0,1:T(8,128)(2,1)S(1)} fusion(bf16[256,4096]{1,0:T(8,128)(2,1)} %reshape.228, bf16[4096,192]{0,1:T(8,128)(2,1)} %get-tuple-element.21, bf16[4096,192]{0,1:T(8,128)(2,1)} %constant_dynamic-update-slice_fusion.5, pred[]{:T(512)S(6)} %eq.2), kind=kOutput, calls=%fused_computation.6 | convolution fusion | flops 403488768 | bytes 5341185 | tf_op jit(solution)/shard_map/dot_general | solution.py:158
  113.4 8.5 %all-to-all-start = ((bf16[128,2,192]{2,1,0:T(2,128)(2,1)}), bf16[128,2,192]{2,1,0:T(2,128)(2,1)S(1)}, u32[]{:S(2)}, u32[]{:S(2)}) async-start(bf16[128,2,192]{2,1,0:T(2,128)(2,1)} %reshape.229), calls=%async_computation | async-start | bytes 262144 | tf_op jit(solution)/shard_map/all_to_all | solution.py:160
  122.1 11.4 %all-to-all-done = bf16[128,2,192]{2,1,0:T(2,128)(2,1)S(1)} async-done(((bf16[128,2,192]{2,1,0:T(2,128)(2,1)}), bf16[128,2,192]{2,1,0:T(2,128)(2,1)S(1)}, u32[]{:S(2)}, u32[]{:S(2)}) %all-to-all-start) | async-done | bytes 98336 | tf_op jit(solution)/shard_map/all_to_all | solution.py:160
  133.7 8.2 %collective-permute-start.1 = (bf16[2,2,64,96]{3,2,1,0:T(8,128)(2,1)S(1)}, bf16[2,2,64,96]{3,2,1,0:T(8,128)(2,1)S(1)}, u32[]{:S(2)}, u32[]{:S(2)}) collective-permute-start(bf16[2,2,64,96]{3,2,1,0:T(8,128)(2,1)S(1)} %get-tuple-element.27), channel_id=1, source_target_pairs={{0,1},{1,0},{2,3},{3,2},{4,5},{5,4},{6,7},{7,6},{8,9},{9,8},{10,11... | collective-permute-start | bytes 147464 | tf_op jit(solution)/shard_map/ppermute | solution.py:21
  141.9 0.8 collective-permute-done.1
  144.1 1.2 fusion.15
  145.7 20.6 %all_gather.10 = bf16[8,2,4,2048]{3,2,1,0:T(4,128)(2,1)} all-gather(bf16[1,2,4,2048]{3,2,1,0:T(4,128)(2,1)S(1)} %broadcast_in_dim_reshape.3), channel_id=1, replica_groups=mesh['dp'=4,'kv_0'=8,'kv_1'=8,'tp'=2] {'kv_0'}, dimensions={0}, use_global_device_ids=true | all-gather | bytes 294912 | tf_op jit(solution)/shard_map/all_gather | solution.py:33
  167.0 37.0 %all-gather.5.cloned.1.call-done = bf16[64,2,4,2048]{3,2,1,0:T(4,128)(2,1)} async-done(((bf16[8,2,4,2048]{3,2,1,0:T(4,128)(2,1)}), bf16[64,2,4,2048]{3,2,1,0:T(4,128)(2,1)}) %all-gather.5.cloned.1.call-update) | async-done | bytes 2097168 | tf_op jit(solution)/shard_map/all_gather | solution.py:33
  204.0 2.7 %copy.110 = bf16[64,2,4,2048]{3,0,2,1:T(8,128)(2,1)S(1)} copy(bf16[64,2,4,2048]{3,2,1,0:T(4,128)(2,1)} %all-gather.5.cloned.1.call-done) | data formatting | bytes 4194304 | tf_op jit(solution)/shard_map/all_gather | solution.py:33
  206.7 2.2 copy.76
  208.9 2.2 dot_general.25
  211.1 2.3 %convolution_convert_fusion = bf16[128,4,64]{0,2,1:T(8,128)(2,1)S(1)} fusion(bf16[128,4,2048]{2,0,1:T(8,128)(2,1)} %dot_general.25, bf16[2048,64]{0,1:T(8,128)(2,1)S(1)} %copy-done), kind=kOutput, calls=%fused_computation.7 | convolution fusion | flops 134250496 | bytes 2424832 | tf_op jit(solution)/shard_map/dot_general | solution.py:195
  213.5 8.3 %all_to_all.20 = bf16[2,128,4,32]{1,3,2,0:T(8,128)(2,1)S(1)} all-to-all(bf16[2,128,4,32]{1,3,2,0:T(8,128)(2,1)S(1)} %bitcast.46), channel_id=1, replica_groups=mesh['dp'=4,'kv_0'=8,'kv_1'=8,'tp'=2] {'tp'}, dimensions={0} | all-to-all | bytes 131072 | tf_op jit(solution)/shard_map/all_to_all | solution.py:51
  (81 shorter events, 10.4 us)
Async XLA Ops:
  7.2 204.0 %copy-start = (bf16[2048,64]{0,1:T(8,128)(2,1)S(1)}, bf16[2048,64]{0,1:T(8,128)(2,1)}, u32[]{:S(2)}) copy-start(bf16[2048,64]{0,1:T(8,128)(2,1)} %param.19) | copy-start | bytes 786436
  7.2 12.5 %copy-start.6 = (bf16[128,4,64]{0,2,1:T(8,128)(2,1)S(1)}, bf16[128,4,64]{0,2,1:T(8,128)(2,1)}, u32[]{:S(2)}) copy-start(bf16[128,4,64]{0,2,1:T(8,128)(2,1)} %param.13) | copy-start | bytes 196612
  7.2 12.6 %copy-start.4 = (bf16[4096,16]{0,1:T(8,128)(2,1)S(1)}, bf16[4096,16]{0,1:T(8,128)(2,1)}, u32[]{:S(2)}) copy-start(bf16[4096,16]{0,1:T(8,128)(2,1)} %param.15) | copy-start | bytes 393220
  7.2 42.9 %copy-start.5 = (bf16[4096,16]{0,1:T(8,128)(2,1)S(1)}, bf16[4096,16]{0,1:T(8,128)(2,1)}, u32[]{:S(2)}) copy-start(bf16[4096,16]{0,1:T(8,128)(2,1)} %param.16) | copy-start | bytes 393220
  7.2 43.6 %copy-start.2 = (bf16[4096,32]{0,1:T(8,128)(2,1)S(1)}, bf16[4096,32]{0,1:T(8,128)(2,1)}, u32[]{:S(2)}) copy-start(bf16[4096,32]{0,1:T(8,128)(2,1)} %param.17) | copy-start | bytes 786436
  7.2 13.2 %copy-start.12 = (s32[2]{0:T(128)S(1)}, s32[2]{0:T(128)}, u32[]{:S(2)}) copy-start(s32[2]{0:T(128)} %param.24) | copy-start | bytes 28
  7.2 13.3 %copy-start.11 = (s32[2]{0:T(128)S(1)}, s32[2]{0:T(128)}, u32[]{:S(2)}) copy-start(s32[2]{0:T(128)} %param.25) | copy-start | bytes 28
  7.2 13.3 %copy-start.13 = (f32[8]{0:T(128)S(1)}, f32[8]{0:T(128)}, u32[]{:S(2)}) copy-start(f32[8]{0:T(128)} %param.20) | copy-start | bytes 100
  7.3 13.6 %copy-start.9 = (bf16[2,4,8,128]{3,2,1,0:T(8,128)(2,1)S(1)}, bf16[2,4,8,128]{3,2,1,0:T(8,128)(2,1)}, u32[]{:S(2)}) copy-start(bf16[2,4,8,128]{3,2,1,0:T(8,128)(2,1)} %param.22) | copy-start | bytes 49156
  7.3 13.7 %copy-start.10 = (bf16[4096]{0:T(1024)(128)(2,1)S(1)}, bf16[4096]{0:T(1024)(128)(2,1)}, u32[]{:S(2)}) copy-start(bf16[4096]{0:T(1024)(128)(2,1)} %param.14) | copy-start | bytes 24580
  7.3 44.3 %copy-start.8 = (bf16[2,4,8,256]{3,2,1,0:T(8,128)(2,1)S(1)}, bf16[2,4,8,256]{3,2,1,0:T(8,128)(2,1)}, u32[]{:S(2)}) copy-start(bf16[2,4,8,256]{3,2,1,0:T(8,128)(2,1)} %param.23) | copy-start | bytes 98308
  7.3 89.1 %all-gather.3.cloned.1.call-start = ((), (), s32[]{:S(2)}) async-start(), calls=%async_computation.2 | async-start | bytes 2129920 | tf_op jit(solution)/shard_map/all_gather | solution.py:143
  11.0 44.2 %collective-permute-start = (bf16[4096,96]{0,1:T(8,128)(2,1)}, bf16[4096,96]{0,1:T(8,128)(2,1)}, u32[]{:S(2)}, u32[]{:S(2)}) collective-permute-start(bf16[4096,96]{0,1:T(8,128)(2,1)} %pad_maximum_fusion), channel_id=1, source_target_pairs={{0,1},{1,0},{2,3},{3,2},{4,5},{5,4},{6,7},{7,6},{8,9},{9,8},{10,11... | collective-permute-start | bytes 2359304 | tf_op jit(solution)/shard_map/ppermute | solution.py:21
  51.5 2.8 %copy-start.3 = (bf16[4096,32]{0,1:T(8,128)(2,1)S(1)}, bf16[4096,32]{0,1:T(8,128)(2,1)}, u32[]{:S(2)}) copy-start(bf16[4096,32]{0,1:T(8,128)(2,1)} %param.18) | copy-start | bytes 786436
  54.4 89.7 %copy-start.1 = (f32[2,8,128,256]{3,2,1,0:T(8,128)}, f32[2,8,128,256]{3,2,1,0:T(8,128)S(1)}, u32[]{:S(2)}) copy-start(f32[2,8,128,256]{3,2,1,0:T(8,128)S(1)} %multiply_add_fusion) | copy-start | bytes 6291460
  113.4 20.1 %all-to-all-start = ((bf16[128,2,192]{2,1,0:T(2,128)(2,1)}), bf16[128,2,192]{2,1,0:T(2,128)(2,1)S(1)}, u32[]{:S(2)}, u32[]{:S(2)}) async-start(bf16[128,2,192]{2,1,0:T(2,128)(2,1)} %reshape.229), calls=%async_computation | async-start | bytes 262144 | tf_op jit(solution)/shard_map/all_to_all | solution.py:160
  122.0 82.0 %all-gather.5.cloned.1.call-start = ((), (), s32[]{:S(2)}) async-start(), calls=%async_computation.3 | async-start | bytes 2359296 | tf_op jit(solution)/shard_map/all_gather | solution.py:33
  133.7 9.1 %collective-permute-start.1 = (bf16[2,2,64,96]{3,2,1,0:T(8,128)(2,1)S(1)}, bf16[2,2,64,96]{3,2,1,0:T(8,128)(2,1)S(1)}, u32[]{:S(2)}, u32[]{:S(2)}) collective-permute-start(bf16[2,2,64,96]{3,2,1,0:T(8,128)(2,1)S(1)} %get-tuple-element.27), channel_id=1, source_target_pairs={{0,1},{1,0},{2,3},{3,2},{4,5},{5,4},{6,7},{7,6},{8,9},{9,8},{10,11... | collective-permute-start | bytes 147464 | tf_op jit(solution)/shard_map/ppermute | solution.py:21
  143.4 2.0 copy-start.7
Sparse Core Ops, SparseCore 0:
  11.7 84.6 all-gather.2
  166.5 37.4 all-gather.4
where the time goes:
time: 230 us; the launch traced here: 229 us
  waiting for transfers between devices  85.2 us (37%)
  blocking collectives  58 us (25%)
  local copies, waits for them, and re-layouts  29.3 us (13%)
  starting transfers between devices  25.6 us (11%)
  between operations  14.4 us (6%)
  matrix products  9.71 us (4%)
  other arithmetic  7.02 us (3%)
    all_gather x1, waiting for transfers between devices, stacked_from(): blocks = lax.all_gather(blocks, axes[k], axis=0, tiled=True)  37 us
    all_gather x1, waiting for transfers between devices, shards(): gathered = lax.all_gather(own_half, KV, axis=2, tiled=True)  36 us
    psum x2, blocking collectives, over_axes(): value = lax.psum(value, axis)  29.1 us
    all_gather x1, blocking collectives, stacked_from(): blocks = lax.all_gather(blocks, axes[k], axis=0, tiled=True)  20.6 us
    ppermute x2, starting transfers between devices, swapped(): lax.ppermute(value, axis, [(i, i ^ 1 << bit) for i in range(lax.axis_size...  16.9 us
    all_to_all x1, waiting for transfers between devices, shards(): lax.all_to_all(columns, KV, split_axis=0, concat_axis=2, tiled=True)  11.4 us
    all_to_all x1, starting transfers between devices, shards(): lax.all_to_all(columns, KV, split_axis=0, concat_axis=2, tiled=True)  8.55 us
    all_to_all x1, blocking collectives, summed_on_arrival(): lax.all_to_all(in_blocks(value, dim, length), axis, 0, 0, tiled=True)  8.27 us
  transfers between devices with their start and end apart: 5, of which 4 were waited for; matrix products, arithmetic and copies ran while one was open for 6% of the time, Pallas kernels for 0%

commit v1 on v0

--- a/solution.py
+++ b/solution.py
@@ -30,7 +30,9 @@
 def stacked_from(value, axes, turns):
     blocks = value[None]
     for k in turns:
-        blocks = lax.all_gather(blocks, axes[k], axis=0, tiled=True)
+        blocks = jnp.concatenate(
+            lax.all_to_all(jnp.stack([blocks] * lax.axis_size(axes[k])), axes[k], 0, 0), axis=0
+        )
     carried = [lax.axis_size(axes[k]) for k in reversed(turns)]
     blocks = blocks.reshape(*carried, *value.shape)
     turned = sorted(range(len(turns)), key=lambda place: turns[len(turns) - 1 - place])

time: 230 us -> 239 us (1.039)
  waiting for transfers between devices: 85.2 us -> 95.7 us
  blocking collectives: 58 us -> 51.3 us
  starting transfers between devices: 25.6 us -> 29.1 us
  local copies, waits for them, and re-layouts: 29.3 us -> 32.3 us
    all_to_all x0 -> x1, waiting for transfers between devices: none -> 47.5 us  [stacked_from(): lax.all_to_all(jnp.stack([blocks] * lax.axis_size(axes[k])), axes[k], 0, 0)]
    all_gather x1 -> x0, waiting for transfers between devices: 37 us -> none  [stacked_from(): blocks = lax.all_gather(blocks, axes[k], axis=0, tiled=True)]
    all_gather x1 -> x0, blocking collectives: 20.6 us -> none  [stacked_from(): blocks = lax.all_gather(blocks, axes[k], axis=0, tiled=True)]
    all_to_all x0 -> x1, blocking collectives: none -> 14.7 us  [stacked_from(): lax.all_to_all(jnp.stack([blocks] * lax.axis_size(axes[k])), axes[k], 0, 0)]
    another operation x1 -> x5, local copies, waits for them, and re-layouts: 0.02 us -> 3.64 us  [stacked_from(): jnp.stack([blocks] * lax.axis_size(axes[k]))]
    all_to_all x0 -> x1, starting transfers between devices: none -> 3.6 us  [stacked_from(): lax.all_to_all(jnp.stack([blocks] * lax.axis_size(axes[k])), axes[k], 0, 0)]
    all_gather x1 -> x0, local copies, waits for them, and re-layouts: 2.74 us -> none  [stacked_from(): blocks = lax.all_gather(blocks, axes[k], axis=0, tiled=True)]
where the time goes in v1:
time: 239 us; the launch traced here: 238 us
  waiting for transfers between devices  95.7 us (40%)
  blocking collectives  51.3 us (21%)
  local copies, waits for them, and re-layouts  32.3 us (14%)
  starting transfers between devices  29.1 us (12%)
  between operations  14.4 us (6%)
  matrix products  8.12 us (3%)
  other arithmetic  7.02 us (3%)
    all_to_all x1, waiting for transfers between devices, stacked_from(): lax.all_to_all(jnp.stack([blocks] * lax.axis_size(axes[k])), axes[k], 0, 0)  47.5 us
    all_gather x1, waiting for transfers between devices, shards(): gathered = lax.all_gather(own_half, KV, axis=2, tiled=True)  36 us
    psum x2, blocking collectives, over_axes(): value = lax.psum(value, axis)  29.1 us
    ppermute x2, starting transfers between devices, swapped(): lax.ppermute(value, axis, [(i, i ^ 1 << bit) for i in range(lax.axis_size...  16.9 us
    all_to_all x1, blocking collectives, stacked_from(): lax.all_to_all(jnp.stack([blocks] * lax.axis_size(axes[k])), axes[k], 0, 0)  14.7 us
    all_to_all x1, waiting for transfers between devices, shards(): lax.all_to_all(columns, KV, split_axis=0, concat_axis=2, tiled=True)  11.5 us
    all_to_all x1, starting transfers between devices, shards(): lax.all_to_all(columns, KV, split_axis=0, concat_axis=2, tiled=True)  8.55 us
    unnamed x37, local copies, waits for them, and re-layouts  8.08 us
  transfers between devices with their start and end apart: 5, of which 4 were waited for; matrix products, arithmetic and copies ran while one was open for 6% of the time, Pallas kernels for 0%

profile of v1, /device:TPU:1, one launch (start us, length us, event | category | flops | bytes accessed | tf_op | source)
XLA Modules:
  0.0 237.9 jit_solution(5030548087370064615)
XLA Ops:
  7.3 1.6 constant_dynamic-slice_fusion
  8.9 2.0 pad_maximum_fusion
  11.0 8.7 %collective-permute-start = (bf16[4096,96]{0,1:T(8,128)(2,1)}, bf16[4096,96]{0,1:T(8,128)(2,1)}, u32[]{:S(2)}, u32[]{:S(2)}) collective-permute-start(bf16[4096,96]{0,1:T(8,128)(2,1)} %pad_maximum_fusion), channel_id=1, source_target_pairs={{0,1},{1,0},{2,3},{3,2},{4,5},{5,4},{6,7},{7,6},{8,9},{9,8},{10,11... | collective-permute-start | bytes 2359304 | tf_op jit(solution)/shard_map/ppermute | solution.py:21
  21.0 14.1 %psum.14 = f32[128,4]{0,1:T(4,128)S(1)} all-reduce(f32[128,4]{0,1:T(4,128)S(1)} %multiply_reduce_fusion), channel_id=1, replica_groups=mesh['dp'=4,'kv_0'=8,'kv_1'=8,'tp'=2] {'kv_0'}, use_global_device_ids=true, to_apply=%region_1.0 | all-reduce | flops 512 | bytes 4096 | tf_op jit(solution)/shard_map/psum | solution.py:16
  35.1 15.0 %psum.15 = f32[128,4]{0,1:T(4,128)S(1)} all-reduce(f32[128,4]{0,1:T(4,128)S(1)} %psum.14), channel_id=1, replica_groups=mesh['dp'=4,'kv_0'=8,'kv_1'=8,'tp'=2] {'kv_1'}, use_global_device_ids=true, to_apply=%region_2.0 | all-reduce | flops 512 | bytes 4096 | tf_op jit(solution)/shard_map/psum | solution.py:16
  51.5 2.8 %multiply_add_fusion = f32[2,8,128,256]{3,2,1,0:T(8,128)S(1)} fusion(f32[2,8,128,256]{3,2,1,0:T(8,128)} %param.21, f32[2,8]{1,0:T(2,128)S(1)} %multiply_exponential_fusion.1, bf16[2,4,8,256]{3,2,1,0:T(8,128)(2,1)S(1)} %copy-done.8, f32[2,4,8,128]{3,2,1,0:T(8,128)S(1)} %convert_multiply_fusion), kind=kOutput, calls=%fused_computation.1 | convolution fusion | flops 26214400 | bytes 4259904 | tf_op jit(solution)/shard_map/sphd,sphe->shde/dot_general | solution.py:83
  55.2 2.5 %constant_dynamic-update-slice_fusion.9 = (bf16[4096,192]{0,1:T(8,128)(2,1)}, bf16[4096,192]{0,1:T(8,128)(2,1)}) fusion(bf16[4096,96]{0,1:T(8,128)(2,1)} %collective-permute-done, bf16[4096,192]{0,1:T(8,128)(2,1)} %constant_dynamic-update-slice_fusion.1), kind=kLoop, calls=%fused_computation.48 | loop fusion | bytes 2359296
  60.4 36.0 %all-gather.2.cloned.1.call-done = bf16[128,2,4096]{0,2,1:T(8,128)(2,1)} async-done(((bf16[128,2,64]{0,2,1:T(8,128)(2,1)}), bf16[128,2,4096]{0,2,1:T(8,128)(2,1)}) %all-gather.2.cloned.1.call-update) | async-done | bytes 2097168 | tf_op jit(solution)/shard_map/all_gather | solution.py:145
  96.4 2.9 %multiply_convert_fusion = bf16[128,2,4096]{0,2,1:T(8,128)(2,1)} fusion(bf16[128,2,4096]{0,2,1:T(8,128)(2,1)} %all-gather.2.cloned.1.call-done, f32[4096]{0:T(1024)S(1)} %convert_element_type.96, f32[128,2]{0,1:T(2,128)S(1)} %add_rsqrt_fusion.1), kind=kLoop, calls=%fused_computation | loop fusion | flops 4194304 | bytes 4211712 | tf_op jit(solution)/shard_map/convert_element_type | solution.py:152
  99.3 6.2 %copy.49 = bf16[128,2,4096]{2,1,0:T(2,128)(2,1)} copy(bf16[128,2,4096]{0,2,1:T(8,128)(2,1)} %multiply_convert_fusion) | data formatting | bytes 4194304 | tf_op jit(solution)/shard_map/convert_element_type | solution.py:152
  105.5 4.1 %reshape.231 = bf16[256,4096]{1,0:T(8,128)(2,1)} reshape(bf16[128,2,4096]{2,1,0:T(2,128)(2,1)} %copy.49) | data formatting | bytes 4194304 | tf_op jit(solution)/shard_map/reshape | solution.py:152
  109.7 2.9 %fusion.3 = bf16[256,192]{0,1:T(8,128)(2,1)S(1)} fusion(bf16[256,4096]{1,0:T(8,128)(2,1)} %reshape.231, bf16[4096,192]{0,1:T(8,128)(2,1)} %get-tuple-element.17, bf16[4096,192]{0,1:T(8,128)(2,1)} %constant_dynamic-update-slice_fusion.5, pred[]{:T(512)S(6)} %eq.2), kind=kOutput, calls=%fused_computation.5 | convolution fusion | flops 403488768 | bytes 5341185 | tf_op jit(solution)/shard_map/dot_general | solution.py:160
  113.4 8.5 %all-to-all-start = ((bf16[128,2,192]{2,1,0:T(2,128)(2,1)}), bf16[128,2,192]{2,1,0:T(2,128)(2,1)S(1)}, u32[]{:S(2)}, u32[]{:S(2)}) async-start(bf16[128,2,192]{2,1,0:T(2,128)(2,1)} %reshape.232), calls=%async_computation | async-start | bytes 262144 | tf_op jit(solution)/shard_map/all_to_all | solution.py:162
  122.1 11.5 %all-to-all-done = bf16[128,2,192]{2,1,0:T(2,128)(2,1)S(1)} async-done(((bf16[128,2,192]{2,1,0:T(2,128)(2,1)}), bf16[128,2,192]{2,1,0:T(2,128)(2,1)S(1)}, u32[]{:S(2)}, u32[]{:S(2)}) %all-to-all-start) | async-done | bytes 98336 | tf_op jit(solution)/shard_map/all_to_all | solution.py:162
  133.6 8.2 %collective-permute-start.1 = (bf16[2,2,64,96]{3,2,1,0:T(8,128)(2,1)S(1)}, bf16[2,2,64,96]{3,2,1,0:T(8,128)(2,1)S(1)}, u32[]{:S(2)}, u32[]{:S(2)}) collective-permute-start(bf16[2,2,64,96]{3,2,1,0:T(8,128)(2,1)S(1)} %get-tuple-element.23), channel_id=1, source_target_pairs={{0,1},{1,0},{2,3},{3,2},{4,5},{5,4},{6,7},{7,6},{8,9},{9,8},{10,11... | collective-permute-start | bytes 147464 | tf_op jit(solution)/shard_map/ppermute | solution.py:21
  141.9 0.8 collective-permute-done.1
  144.1 1.2 fusion.15
  145.9 14.7 %all_to_all.30 = bf16[8,1,2,4,2048]{4,2,3,1,0:T(2,128)(2,1)S(1)} all-to-all(bf16[8,1,2,4,2048]{4,2,3,1,0:T(2,128)(2,1)S(1)} %stack.6), channel_id=1, replica_groups=mesh['dp'=4,'kv_0'=8,'kv_1'=8,'tp'=2] {'kv_0'}, dimensions={0} | all-to-all | bytes 524288 | tf_op jit(solution)/shard_map/all_to_all | solution.py:34
  160.8 3.2 %stack.7 = bf16[8,8,2,4,2048]{4,2,1,3,0:T(2,128)(2,1)} broadcast(bf16[8,2,4,2048]{3,1,0,2:T(2,128)(2,1)S(1)} %copy.62), dimensions={1,2,3,4} | broadcast | bytes 2359296 | tf_op jit(solution)/shard_map/stack | solution.py:34
  164.1 3.6 %all-to-all-start.2 = ((bf16[8,8,2,4,2048]{4,2,1,3,0:T(2,128)(2,1)}), bf16[8,8,2,4,2048]{4,2,1,3,0:T(2,128)(2,1)S(1)}, u32[]{:S(2)}, u32[]{:S(2)}) async-start(bf16[8,8,2,4,2048]{4,2,1,3,0:T(2,128)(2,1)} %stack.7), calls=%async_computation.2 | async-start | bytes 4194304 | tf_op jit(solution)/shard_map/all_to_all | solution.py:34
  168.3 47.5 %all-to-all-done.2 = bf16[8,8,2,4,2048]{4,2,1,3,0:T(2,128)(2,1)S(1)} async-done(((bf16[8,8,2,4,2048]{4,2,1,3,0:T(2,128)(2,1)}), bf16[8,8,2,4,2048]{4,2,1,3,0:T(2,128)(2,1)S(1)}, u32[]{:S(2)}, u32[]{:S(2)}) %all-to-all-start.2) | async-done | bytes 2097184 | tf_op jit(solution)/shard_map/all_to_all | solution.py:34
  215.7 3.7 %copy.63 = bf16[8,8,2,4,2048]{4,2,1,0,3:T(2,128)(2,1)} copy(bf16[8,8,2,4,2048]{4,2,0,3,1:T(2,128)(2,1)S(1)} %bitcast.39) | data formatting | bytes 4194304 | tf_op jit(solution)/shard_map/transpose | solution.py:39
  219.5 2.7 %dot_general.25 = bf16[128,4,2048]{2,0,1:T(8,128)(2,1)S(1)} reshape(bf16[8,8,2,4,2048]{4,2,1,0,3:T(2,128)(2,1)} %copy.63) | data formatting | bytes 4194304 | tf_op jit(solution)/shard_map/dot_general | solution.py:197
  223.0 7.4 %all_to_all.31 = bf16[2,128,4,32]{1,3,2,0:T(8,128)(2,1)S(1)} all-to-all(bf16[2,128,4,32]{1,3,2,0:T(8,128)(2,1)S(1)} %bitcast.44), channel_id=1, replica_groups=mesh['dp'=4,'kv_0'=8,'kv_1'=8,'tp'=2] {'tp'}, dimensions={0} | all-to-all | bytes 131072 | tf_op jit(solution)/shard_map/all_to_all | solution.py:53
  (83 shorter events, 11.4 us)
Async XLA Ops:
  7.2 215.1 %copy-start = (bf16[2048,64]{0,1:T(8,128)(2,1)S(1)}, bf16[2048,64]{0,1:T(8,128)(2,1)}, u32[]{:S(2)}) copy-start(bf16[2048,64]{0,1:T(8,128)(2,1)} %param.19) | copy-start | bytes 786436
  7.2 12.5 %copy-start.6 = (bf16[128,4,64]{0,2,1:T(8,128)(2,1)S(1)}, bf16[128,4,64]{0,2,1:T(8,128)(2,1)}, u32[]{:S(2)}) copy-start(bf16[128,4,64]{0,2,1:T(8,128)(2,1)} %param.13) | copy-start | bytes 196612
  7.2 12.6 %copy-start.4 = (bf16[4096,16]{0,1:T(8,128)(2,1)S(1)}, bf16[4096,16]{0,1:T(8,128)(2,1)}, u32[]{:S(2)}) copy-start(bf16[4096,16]{0,1:T(8,128)(2,1)} %param.15) | copy-start | bytes 393220
  7.2 42.9 %copy-start.5 = (bf16[4096,16]{0,1:T(8,128)(2,1)S(1)}, bf16[4096,16]{0,1:T(8,128)(2,1)}, u32[]{:S(2)}) copy-start(bf16[4096,16]{0,1:T(8,128)(2,1)} %param.16) | copy-start | bytes 393220
  7.2 43.6 %copy-start.2 = (bf16[4096,32]{0,1:T(8,128)(2,1)S(1)}, bf16[4096,32]{0,1:T(8,128)(2,1)}, u32[]{:S(2)}) copy-start(bf16[4096,32]{0,1:T(8,128)(2,1)} %param.17) | copy-start | bytes 786436
  7.2 13.2 %copy-start.12 = (s32[2]{0:T(128)S(1)}, s32[2]{0:T(128)}, u32[]{:S(2)}) copy-start(s32[2]{0:T(128)} %param.24) | copy-start | bytes 28
  7.2 13.3 %copy-start.11 = (s32[2]{0:T(128)S(1)}, s32[2]{0:T(128)}, u32[]{:S(2)}) copy-start(s32[2]{0:T(128)} %param.25) | copy-start | bytes 28
  7.2 13.3 %copy-start.13 = (f32[8]{0:T(128)S(1)}, f32[8]{0:T(128)}, u32[]{:S(2)}) copy-start(f32[8]{0:T(128)} %param.20) | copy-start | bytes 100
  7.3 13.6 %copy-start.9 = (bf16[2,4,8,128]{3,2,1,0:T(8,128)(2,1)S(1)}, bf16[2,4,8,128]{3,2,1,0:T(8,128)(2,1)}, u32[]{:S(2)}) copy-start(bf16[2,4,8,128]{3,2,1,0:T(8,128)(2,1)} %param.22) | copy-start | bytes 49156
  7.3 13.7 %copy-start.10 = (bf16[4096]{0:T(1024)(128)(2,1)S(1)}, bf16[4096]{0:T(1024)(128)(2,1)}, u32[]{:S(2)}) copy-start(bf16[4096]{0:T(1024)(128)(2,1)} %param.14) | copy-start | bytes 24580
  7.3 44.3 %copy-start.8 = (bf16[2,4,8,256]{3,2,1,0:T(8,128)(2,1)S(1)}, bf16[2,4,8,256]{3,2,1,0:T(8,128)(2,1)}, u32[]{:S(2)}) copy-start(bf16[2,4,8,256]{3,2,1,0:T(8,128)(2,1)} %param.23) | copy-start | bytes 98308
  7.3 89.1 %all-gather.2.cloned.1.call-start = ((), (), s32[]{:S(2)}) async-start(), calls=%async_computation.4 | async-start | bytes 2129920 | tf_op jit(solution)/shard_map/all_gather | solution.py:145
  11.0 44.2 %collective-permute-start = (bf16[4096,96]{0,1:T(8,128)(2,1)}, bf16[4096,96]{0,1:T(8,128)(2,1)}, u32[]{:S(2)}, u32[]{:S(2)}) collective-permute-start(bf16[4096,96]{0,1:T(8,128)(2,1)} %pad_maximum_fusion), channel_id=1, source_target_pairs={{0,1},{1,0},{2,3},{3,2},{4,5},{5,4},{6,7},{7,6},{8,9},{9,8},{10,11... | collective-permute-start | bytes 2359304 | tf_op jit(solution)/shard_map/ppermute | solution.py:21
  51.5 2.8 %copy-start.3 = (bf16[4096,32]{0,1:T(8,128)(2,1)S(1)}, bf16[4096,32]{0,1:T(8,128)(2,1)}, u32[]{:S(2)}) copy-start(bf16[4096,32]{0,1:T(8,128)(2,1)} %param.18) | copy-start | bytes 786436
  54.4 89.7 %copy-start.1 = (f32[2,8,128,256]{3,2,1,0:T(8,128)}, f32[2,8,128,256]{3,2,1,0:T(8,128)S(1)}, u32[]{:S(2)}) copy-start(f32[2,8,128,256]{3,2,1,0:T(8,128)S(1)} %multiply_add_fusion) | copy-start | bytes 6291460
  113.4 20.1 %all-to-all-start = ((bf16[128,2,192]{2,1,0:T(2,128)(2,1)}), bf16[128,2,192]{2,1,0:T(2,128)(2,1)S(1)}, u32[]{:S(2)}, u32[]{:S(2)}) async-start(bf16[128,2,192]{2,1,0:T(2,128)(2,1)} %reshape.232), calls=%async_computation | async-start | bytes 262144 | tf_op jit(solution)/shard_map/all_to_all | solution.py:162
  133.6 9.1 %collective-permute-start.1 = (bf16[2,2,64,96]{3,2,1,0:T(8,128)(2,1)S(1)}, bf16[2,2,64,96]{3,2,1,0:T(8,128)(2,1)S(1)}, u32[]{:S(2)}, u32[]{:S(2)}) collective-permute-start(bf16[2,2,64,96]{3,2,1,0:T(8,128)(2,1)S(1)} %get-tuple-element.23), channel_id=1, source_target_pairs={{0,1},{1,0},{2,3},{3,2},{4,5},{5,4},{6,7},{7,6},{8,9},{9,8},{10,11... | collective-permute-start | bytes 147464 | tf_op jit(solution)/shard_map/ppermute | solution.py:21
  143.4 2.0 copy-start.7
  164.1 51.7 %all-to-all-start.2 = ((bf16[8,8,2,4,2048]{4,2,1,3,0:T(2,128)(2,1)}), bf16[8,8,2,4,2048]{4,2,1,3,0:T(2,128)(2,1)S(1)}, u32[]{:S(2)}, u32[]{:S(2)}) async-start(bf16[8,8,2,4,2048]{4,2,1,3,0:T(2,128)(2,1)} %stack.7), calls=%async_computation.2 | async-start | bytes 4194304 | tf_op jit(solution)/shard_map/all_to_all | solution.py:34
Sparse Core Ops, SparseCore 0:
  11.7 84.6 all-gather.1
